TPU v7x, 32 devices: a whole 2x2x4 slice. The times are simulated.
32 devices in a mesh: grp: 2 (over x), tp: 4 (over z), dp: 4 (over y, core).
Axes of the slice: x: 2, y: 2, z: 4, core: 2. Of those that a mesh axis runs over, the one named last changes fastest.
Arguments:
- tokens: bfloat16 [32, 4096], P(('grp', 'tp'), 'dp'), parts along dimension 0, may hold values from -30 to 30
- norm_gain: float32 [2, 4096], P(None, 'dp'), may hold values from 0.1 to 1.9
- w_query: bfloat16 [2, 4096, 2048], P(None, 'dp', 'tp'), may hold values from -0.09375 to 0.09375
- w_forget: bfloat16 [2, 4096, 2048], P(None, 'dp', 'tp'), may hold values from -0.09375 to 0.09375
- w_value: bfloat16 [2, 4096, 2048], P(None, 'dp', 'tp'), may hold values from -0.09375 to 0.09375
- w_gate: bfloat16 [2, 4096, 2048], P(None, 'dp', 'tp'), may hold values from -0.09375 to 0.09375
- lower_bound: float32 [2, 2048], P(None, 'tp'), may hold values from 0 to 0.9
- head_gain: float32 [2, 128], replicated, may hold values from 0.1 to 1.9
- w_out: bfloat16 [2, 2048, 4096], P(None, 'tp', 'dp'), may hold values from -0.125 to 0.125
- state: float32 [2, 32, 16, 128, 128], P(None, ('grp', 'dp'), 'tp'), parts along dimension 1, may hold values from -4 to 4
Outputs:
- hidden_out: bfloat16 [32, 4096], P(('grp', 'tp'), 'dp'), parts along dimension 0
- new_state: float32 [2, 32, 16, 128, 128], P(None, ('grp', 'dp'), 'tp'), parts along dimension 1
There are 2 independent parts, one for each index of `grp`. A program takes and returns all parts, laid end to end along the dimension named above; an argument that names none is the same for every part. Nothing has to cross between parts.
All inputs are finite; a program needn't handle non-finite values.
Results may differ from a plain program's by a relative error of at most 0.02.
Values may be sent and summed in bfloat16 or wider, within the bound.
A program may use at most 64 MiB of HBM per device.

v0:
```python
import jax
import jax.numpy as jnp
from jax import lax
from jax.sharding import PartitionSpec as P

D = 4096
HD = 128


def per_device(
    tokens, norm_gain, w_query, w_forget, w_value, w_gate, lower_bound, head_gain, w_out, state
):
    local_seqs = state.shape[1]
    head_count = state.shape[2]
    offset = lax.axis_index("dp") * local_seqs
    hidden = tokens
    updated = []
    for layer in range(2):
        gathered = lax.all_gather(hidden, "tp", axis=0, tiled=True)
        widened = gathered.astype(jnp.float32)
        squares = jnp.sum(widened * widened, axis=1)
        scaled = (widened * norm_gain[layer]).astype(jnp.bfloat16)
        joined = jnp.concatenate(
            [
                jnp.dot(scaled, weight[layer], preferred_element_type=jnp.float32)
                for weight in (w_query, w_forget, w_value, w_gate)
            ],
            axis=1,
        )
        square_total = lax.psum(squares, "dp")
        own_squares = lax.dynamic_slice_in_dim(square_total, offset, local_seqs, 0)
        payload = (joined,)
        summed = (lax.psum(payload[0].astype(jnp.bfloat16), "dp").astype(jnp.float32),)
        shares = tuple(
            (lax.dynamic_slice_in_dim(member, offset, local_seqs, 0) for member in summed)
        )
        own_proj = shares[0]
        width = own_proj.shape[1] // 4
        factor = lax.rsqrt(own_squares / D + 1e-06)[:, None]
        query, forget_pre, value, gate_pre = (
            own_proj[:, index * width : (index + 1) * width] * factor for index in range(4)
        )
        bound = lower_bound[layer]
        forget = bound + (1.0 - bound) * jax.nn.sigmoid(forget_pre)
        keyvec = (1.0 - bound) * jax.nn.sigmoid(-forget_pre)

        def shaped(array):
            return array.reshape(local_seqs, head_count, HD)

        carried = (
            shaped(forget)[..., None] * state[layer]
            + shaped(keyvec)[..., None] * shaped(value)[..., None, :]
        )
        updated.append(carried)
        readout = jnp.einsum("bhkv,bhk->bhv", carried, shaped(query))
        readout = (
            readout
            * lax.rsqrt(jnp.mean(readout * readout, axis=-1, keepdims=True) + 1e-06)
            * head_gain[layer]
        )
        normed = (readout.reshape(local_seqs, head_count * HD) * jax.nn.sigmoid(gate_pre)).astype(
            jnp.bfloat16
        )
        out_weight = w_out[layer]
        mixed = jnp.dot(
            lax.all_gather(normed, "dp", axis=0, tiled=True),
            out_weight,
            preferred_element_type=jnp.float32,
        )
        mixed_sum = lax.psum_scatter(
            mixed.astype(jnp.bfloat16), "tp", scatter_dimension=0, tiled=True
        ).astype(jnp.float32)
        hidden = (hidden.astype(jnp.float32) + mixed_sum).astype(jnp.bfloat16)
    return (hidden, jnp.stack(updated))


def solution(mesh):
    return jax.shard_map(
        per_device,
        mesh=mesh,
        in_specs=(
            P(("grp", "tp"), "dp"),
            P(None, "dp"),
            P(None, "dp", "tp"),
            P(None, "dp", "tp"),
            P(None, "dp", "tp"),
            P(None, "dp", "tp"),
            P(None, "tp"),
            P(),
            P(None, "tp", "dp"),
            P(None, ("grp", "dp"), "tp", None, None),
        ),
        out_specs=(P(("grp", "tp"), "dp"), P(None, ("grp", "dp"), "tp", None, None)),
        check_vma=False,
    )
```

profile of v0, /device:TPU:0, one launch (start us, length us, event | category | flops | bytes accessed | tf_op | source)
XLA Modules:
  0.0 181.9 jit_solution(1064112044140529132)
XLA Ops:
  7.2 0.9 fusion.47
  8.1 15.1 %all-gather = bf16[4,4,1024]{2,1,0:T(4,128)(2,1)S(1)} all-gather(bf16[1,4,1024]{2,1,0:T(4,128)(2,1)} %bitcast.92), channel_id=1, replica_groups=mesh['grp'=2,'tp'=4,'dp'=4] {'tp'}, dimensions={0}, use_global_device_ids=true | all-gather | bytes 40960 | tf_op jit(solution)/shard_map/all_gather | solution.py:19
  23.2 0.1 multiply_convert_fusion.1
  23.3 1.5 convolution_convert_fusion.6
  24.8 1.5 convolution_convert_fusion.7
  26.3 0.3 convolution_convert_fusion.8
  26.5 1.6 convolution_convert_fusion.9
  28.2 0.7 pad_maximum_fusion.1
  28.9 5.7 %psum.29 = f32[16]{0:T(128)S(1)} all-reduce(f32[16]{0:T(128)S(1)} %get-tuple-element.7), channel_id=1, replica_groups=mesh['grp'=2,'tp'=4,'dp'=4] {'dp'}, use_global_device_ids=true, to_apply=%region_2.0 | all-reduce | flops 16 | bytes 128 | tf_op jit(solution)/shard_map/psum | solution.py:30
  34.7 0.6 dynamic-slice
  35.9 25.6 %all-reduce.5.cloned.1.call-done = bf16[16,2048]{1,0:T(8,128)(2,1)} async-done(((bf16[16,2048]{1,0:T(8,128)(2,1)}), bf16[16,2048]{1,0:T(8,128)(2,1)}) %all-reduce.5.cloned.1.call-update) | async-done | bytes 65552 | tf_op jit(solution)/shard_map/psum | solution.py:33
  61.5 0.8 dynamic-slice_convert_fusion.1
  62.4 1.9 %fusion.10 = f32[4,4,1,128]{3,2,1,0:T(1,128)S(1)} fusion(f32[4,4,128,1]{2,3,1,0:T(1,128)S(1)} %bitcast.100, f32[2,4,4,128,128]{4,3,2,1,0:T(8,128)} %param.19, f32[4,4,128]{2,1,0:T(4,128)S(1)} %mul.268, f32[4,4,128]{2,1,0:T(4,128)S(1)} %mul.265, f32[4,4,128]{2,1,0:T(4,128)S(1)} %mul.261), kind=kOutput, calls=%fused_computation.22 | convolution fusion | flops 1310720 | bytes 1089536 | tf_op jit(solution)/shard_map/bhkv,bhk->bhv/dot_general | solution.py:55
  64.6 5.2 %all-gather.1 = bf16[4,4,512]{2,1,0:T(4,128)(2,1)S(1)} all-gather(bf16[1,4,512]{2,1,0:T(4,128)(2,1)S(1)} %fusion.45), channel_id=1, replica_groups=mesh['grp'=2,'tp'=4,'dp'=4] {'dp'}, dimensions={0}, use_global_device_ids=true | all-gather | bytes 20480 | tf_op jit(solution)/shard_map/all_gather | solution.py:66
  69.9 1.5 convolution_convert_fusion.1
  71.3 19.0 %all-reduce = bf16[16,1024]{1,0:T(8,128)(2,1)S(1)} all-reduce(bf16[16,1024]{1,0:T(8,128)(2,1)S(1)} %convolution_convert_fusion.1), channel_id=2, replica_groups=mesh['grp'=2,'tp'=4,'dp'=4] {'tp'}, use_global_device_ids=true, to_apply=%region_4.0.clone | all-reduce | flops 16384 | bytes 65536
  90.4 13.1 %all-gather.2 = bf16[4,4,1024]{2,1,0:T(4,128)(2,1)S(1)} all-gather(bf16[1,4,1024]{2,1,0:T(4,128)(2,1)S(1)} %fusion.46), channel_id=1, replica_groups=mesh['grp'=2,'tp'=4,'dp'=4] {'tp'}, dimensions={0}, use_global_device_ids=true | all-gather | bytes 40960 | tf_op jit(solution)/shard_map/all_gather | solution.py:19
  103.6 0.2 convolution_convert_fusion.2
  103.9 1.7 convolution_convert_fusion.3
  105.6 0.3 convolution_convert_fusion.4
  105.8 1.5 convolution_convert_fusion.5
  107.3 5.9 %psum.31 = f32[16]{0:T(128)S(1)} all-reduce(f32[16]{0:T(128)S(1)} %get-tuple-element.5), channel_id=1, replica_groups=mesh['grp'=2,'tp'=4,'dp'=4] {'dp'}, use_global_device_ids=true, to_apply=%region_7.0 | all-reduce | flops 16 | bytes 128 | tf_op jit(solution)/shard_map/psum | solution.py:30
  113.1 0.6 pad_maximum_fusion.2
  113.9 28.8 %all-reduce.7.cloned.1.call-done = bf16[16,2048]{1,0:T(8,128)(2,1)} async-done(((bf16[16,2048]{1,0:T(8,128)(2,1)}), bf16[16,2048]{1,0:T(8,128)(2,1)}) %all-reduce.7.cloned.1.call-update) | async-done | bytes 65552 | tf_op jit(solution)/shard_map/psum | solution.py:33
  142.7 0.8 dynamic-slice_convert_fusion
  143.7 2.6 %multiply_add_fusion.1 = (f32[1,4,4,128,128]{4,3,2,1,0:T(8,128)S(1)}, f32[1,4,4,128,128]{4,3,2,1,0:T(8,128)S(1)}) fusion(f32[2,4,4,128,128]{4,3,2,1,0:T(8,128)} %param.19, f32[4,4,128]{2,1,0:T(4,128)S(1)} %mul.268, f32[4,4,128]{2,1,0:T(4,128)S(1)} %mul.265, f32[4,4,128]{2,1,0:T(4,128)S(1)} %mul.261, f32[4,4,128]{2,1,0:T(4,128)S(1)} %mul.296, ...), kind=kLoop, calls=%fused_computation.28 | loop fusion | flops 1572864 | bytes 4243456 | tf_op jit(solution)/shard_map/add | solution.py:51
  146.3 0.7 fusion.2
  147.3 5.2 %all-gather.3 = bf16[4,4,512]{2,1,0:T(4,128)(2,1)S(1)} all-gather(bf16[1,4,512]{2,1,0:T(4,128)(2,1)S(1)} %fusion.44), channel_id=1, replica_groups=mesh['grp'=2,'tp'=4,'dp'=4] {'dp'}, dimensions={0}, use_global_device_ids=true | all-gather | bytes 20480 | tf_op jit(solution)/shard_map/all_gather | solution.py:66
  152.5 1.5 convolution_convert_fusion
  154.0 19.0 %all-reduce.1 = bf16[16,1024]{1,0:T(8,128)(2,1)S(1)} all-reduce(bf16[16,1024]{1,0:T(8,128)(2,1)S(1)} %convolution_convert_fusion), channel_id=3, replica_groups=mesh['grp'=2,'tp'=4,'dp'=4] {'tp'}, use_global_device_ids=true, to_apply=%region_9.0.clone | all-reduce | flops 16384 | bytes 65536
  173.0 0.6 add_convert_fusion
  173.6 1.5 pad_maximum_fusion
  (48 shorter events, 1.3 us)
Async XLA Ops:
  7.2 19.1 %copy-start.1 = (bf16[2,1024,512]{2,1,0:T(8,128)(2,1)S(1)}, bf16[2,1024,512]{2,1,0:T(8,128)(2,1)}, u32[]{:S(2)}) copy-start(bf16[2,1024,512]{2,1,0:T(8,128)(2,1)} %param.13) | copy-start | bytes 6291460
  7.2 54.3 %all-reduce.5.cloned.1.call-start = ((), (), s32[]{:S(2)}) async-start(), calls=%async_computation | async-start | bytes 131072 | tf_op jit(solution)/shard_map/psum | solution.py:33
  23.3 5.6 %copy-start.6 = (f32[2,128]{1,0:T(2,128)S(1)}, f32[2,128]{1,0:T(2,128)}, u32[]{:S(2)}) copy-start(f32[2,128]{1,0:T(2,128)} %param.17) | copy-start | bytes 3076
  23.3 5.6 %copy-start.5 = (f32[2,512]{1,0:T(2,128)S(1)}, f32[2,512]{1,0:T(2,128)}, u32[]{:S(2)}) copy-start(f32[2,512]{1,0:T(2,128)} %param.16) | copy-start | bytes 12292
  23.3 11.4 %copy-start.7 = (u32[32]{0:T(128)S(1)}, u32[32]{0:T(128)}, u32[]{:S(2)}) copy-start(u32[32]{0:T(128)} %constant.30) | copy-start | bytes 388
  26.5 63.8 %copy-start.4 = (bf16[4,1024]{1,0:T(4,128)(2,1)S(1)}, bf16[4,1024]{1,0:T(4,128)(2,1)}, u32[]{:S(2)}) copy-start(bf16[4,1024]{1,0:T(4,128)(2,1)} %param.10) | copy-start | bytes 24580
  26.5 77.1 %copy-start = (bf16[2,1024,512]{2,1,0:T(8,128)(2,1)S(1)}, bf16[2,1024,512]{2,1,0:T(8,128)(2,1)}, u32[]{:S(2)}) copy-start(bf16[2,1024,512]{2,1,0:T(8,128)(2,1)} %param.15) | copy-start | bytes 6291460
  28.8 113.9 %all-reduce.7.cloned.1.call-start = ((), (), s32[]{:S(2)}) async-start(), calls=%async_computation.1 | async-start | bytes 131072 | tf_op jit(solution)/shard_map/psum | solution.py:33
  103.5 2.1 %copy-start.2 = (bf16[2,1024,512]{2,1,0:T(8,128)(2,1)S(1)}, bf16[2,1024,512]{2,1,0:T(8,128)(2,1)}, u32[]{:S(2)}) copy-start(bf16[2,1024,512]{2,1,0:T(8,128)(2,1)} %param.13) | copy-start | bytes 6291460
  143.7 2.6 %copy-start.3 = (f32[2,4,4,128,128]{4,3,2,1,0:T(8,128)S(1)}, f32[2,4,4,128,128]{4,3,2,1,0:T(8,128)}, u32[]{:S(2)}) copy-start(f32[2,4,4,128,128]{4,3,2,1,0:T(8,128)} %param.19) | copy-start | bytes 6291460
Sparse Core Ops, SparseCore 0:
  28.9 32.5 all-reduce.4
  113.9 28.7 all-reduce.6
where the time goes:
time: 182 us
  blocking collectives  88.1 us (48%)
  waiting for transfers between devices  54.5 us (30%)
  between operations  14.9 us (8%)
  matrix products  14.1 us (8%)
  other arithmetic  8.64 us (5%)
    psum x2, waiting for transfers between devices, per_device(): lax.psum(payload[0].astype(jnp.bfloat16), 'dp').astype(jnp.float32)  54.4 us
    unnamed x2, blocking collectives  38 us
    all_gather x2, blocking collectives, per_device(): gathered = lax.all_gather(hidden, 'tp', axis=0, tiled=True)  28.2 us
    psum x2, blocking collectives, per_device(): square_total = lax.psum(squares, 'dp')  11.5 us
    all_gather x2, blocking collectives, per_device(): lax.all_gather(normed, 'dp', axis=0, tiled=True)  10.4 us
    dot_general x8, matrix products, per_device(): jnp.dot(scaled, weight[layer], preferred_element_type=jnp.float32)  8.47 us
  transfers between devices with their start and end apart: 2, of which 2 were waited for; matrix products, arithmetic and copies ran while one was open for 0% of the time, Pallas kernels for 0%

commit v1 on v0

v1 whole, which is shorter than its diff:
```python
import functools

import jax
import jax.numpy as jnp
from jax import lax
from jax.experimental import pallas as pl
from jax.experimental.pallas import tpu as pltpu
from jax.sharding import PartitionSpec as P

MESH = pl.DeviceIdType.MESH
LANES = 128
F32 = jnp.float32
BF16 = jnp.bfloat16


def each(count, body):
    if count <= 8:
        for d in range(1, count):
            body(d)
    else:

        @pl.loop(1, count)
        def _(d):
            body(d)


def kernel(
    tp, dp,
    tok, gain, wq, wf, wv, wg, bound_ref, head_gain, wo, st,
    out, ns,
    w_v, wo_v, s_v, xg, hf, h3, sq2, sqs, sqr, pf, ps, pr, tr_a, tr_b, ro,
    na, nf, po, ar, rs, rr,
    w_sem, wo_sem, s_sem, o_sem, xg_s, xg_r, sq_s, sq_r, p_s, p_r, n_s, n_r,
    ar_s, ar_r, rs_s, rs_r,
):
    rows, cols = tok.shape
    seqs, heads, hd = st.shape[1], st.shape[2], st.shape[3]
    width = wq.shape[2]
    pairs = seqs * heads
    features = cols * dp
    me_tp = lax.axis_index("tp")
    me_dp = lax.axis_index("dp")

    def remote(src, dst, send, recv, axis, peer):
        return pltpu.make_async_remote_copy(
            src_ref=src, dst_ref=dst, send_sem=send, recv_sem=recv,
            device_id={axis: peer}, device_id_type=MESH,
        )

    weights = (wq, wf, wv, wg)

    def load_w(l, i):
        return pltpu.make_async_copy(weights[i].at[l], w_v.at[l, i], w_sem.at[l, i])

    def load_wo(l):
        return pltpu.make_async_copy(wo.at[l], wo_v.at[l], wo_sem.at[l])

    def load_s(l):
        return pltpu.make_async_copy(st.at[l], s_v.at[l], s_sem.at[l])

    def store_s(l):
        return pltpu.make_async_copy(s_v.at[l], ns.at[l], o_sem.at[l])

    for l in range(2):
        for i in range(4):
            load_w(l, i).start()
        load_s(l).start()
        load_wo(l).start()

    barrier = pltpu.get_barrier_semaphore()

    def greet_tp(d):
        pl.semaphore_signal(
            barrier, inc=1, device_id={"tp": lax.rem(me_tp + d, tp)}, device_id_type=MESH
        )

    def greet_dp(d):
        pl.semaphore_signal(
            barrier, inc=1, device_id={"dp": lax.rem(me_dp + d, dp)}, device_id_type=MESH
        )

    each(tp, greet_tp)
    each(dp, greet_dp)
    pl.semaphore_wait(barrier, tp + dp - 2)

    def xg_copy(d):
        return remote(tok, xg.at[me_tp], xg_s.at[d], xg_r.at[me_tp], "tp", lax.rem(me_tp + d, tp))

    each(tp, lambda d: xg_copy(d).start())
    xg[me_tp] = tok[...]

    def xg_wait(d):
        src = lax.rem(me_tp + tp - d, tp)
        remote(tok, xg.at[src], xg_s.at[d], xg_r.at[src], "tp", src).wait_recv()

    each(tp, xg_wait)
    for j in range(tp):
        hf[j * rows:(j + 1) * rows, :] = xg[j].astype(F32)

    for l in range(2):
        h = hf[...]
        sq2[...] = jnp.broadcast_to(
            jnp.sum(h * h, axis=1, keepdims=True), (h.shape[0], LANES)
        )
        for j in range(dp):
            sqs[l, j] = sq2[j * seqs:(j + 1) * seqs, :]

        def sq_copy(d):
            peer = lax.rem(me_dp + d, dp)
            return remote(
                sqs.at[l, peer], sqr.at[l, me_dp], sq_s.at[l, d], sq_r.at[l, me_dp], "dp", peer
            )

        each(dp, lambda d: sq_copy(d).start())
        scaled = (h * gain[l:l + 1, :]).astype(BF16)

        def p_copy(i, d):
            peer = lax.rem(me_dp + d, dp)
            return remote(
                ps.at[l, i, peer], pr.at[l, i, me_dp], p_s.at[l, i, d], p_r.at[l, i, me_dp],
                "dp", peer,
            )

        for i in range(4):
            load_w(l, i).wait()
            pf[i] = jnp.dot(scaled, w_v[l, i], preferred_element_type=F32)
            for j in range(dp):
                ps[l, i, j] = pf[i, j * seqs:(j + 1) * seqs, :].astype(BF16)
            each(dp, lambda d: p_copy(i, d).start())

        def sq_wait(d):
            src = lax.rem(me_dp + dp - d, dp)
            remote(
                sqs.at[l, src], sqr.at[l, src], sq_s.at[l, d], sq_r.at[l, src], "dp", src
            ).wait_recv()

        sqr[l, me_dp] = sqs[l, me_dp]
        each(dp, sq_wait)
        total = sqr[l, 0]
        for j in range(1, dp):
            total = total + sqr[l, j]
        factor = lax.rsqrt(total / features + 1e-06)

        load_s(l).wait()
        proj = []
        for i in range(4):

            def p_wait(d):
                src = lax.rem(me_dp + dp - d, dp)
                remote(
                    ps.at[l, i, src], pr.at[l, i, src], p_s.at[l, i, d], p_r.at[l, i, src],
                    "dp", src,
                ).wait_recv()

            pr[l, i, me_dp] = ps[l, i, me_dp]
            each(dp, p_wait)
            acc = pr[l, i, 0].astype(F32)
            for j in range(1, dp):
                acc = acc + pr[l, i, j].astype(F32)
            proj.append(acc)

        values, dots, gates = [], [], []
        for k in range(heads):
            lanes = slice(k * hd, (k + 1) * hd)
            query, forget_pre, value, gate_pre = (proj[i][:, lanes] * factor for i in range(4))
            bound = bound_ref[l:l + 1, lanes]
            forget = bound + (1.0 - bound) * jax.nn.sigmoid(forget_pre)
            keyvec = (1.0 - bound) * jax.nn.sigmoid(-forget_pre)
            tr_a[k * seqs:(k + 1) * seqs, :] = forget * query
            tr_b[k * seqs:(k + 1) * seqs, :] = forget
            tr_b[pairs + k * seqs:pairs + (k + 1) * seqs, :] = keyvec
            values.append(value)
            dots.append(jnp.sum(query * keyvec, axis=1, keepdims=True) * value)
            gates.append(jax.nn.sigmoid(gate_pre))
        cols_a = tr_a[...].T
        for k in range(heads):
            for b in range(seqs):
                p = k * seqs + b
                ro[p:p + 1, :] = jnp.sum(cols_a[:, p:p + 1] * s_v[l, b, k], axis=0, keepdims=True)
        for k in range(heads):
            readout = ro[k * seqs:(k + 1) * seqs, :] + dots[k]
            readout = (
                readout
                * lax.rsqrt(jnp.mean(readout * readout, axis=-1, keepdims=True) + 1e-06)
                * head_gain[l:l + 1, :]
            )
            na[l, me_dp, :, k * hd:(k + 1) * hd] = (readout * gates[k]).astype(BF16)

        def n_copy(d):
            peer = lax.rem(me_dp + d, dp)
            return remote(
                na.at[l, me_dp], na.at[l, me_dp], n_s.at[l, d], n_r.at[l, me_dp], "dp", peer
            )

        each(dp, lambda d: n_copy(d).start())

        cols_b = tr_b[...].T
        for k in range(heads):
            for b in range(seqs):
                p = k * seqs + b
                s_v[l, b, k] = (
                    cols_b[:, p:p + 1] * s_v[l, b, k]
                    + cols_b[:, pairs + p:pairs + p + 1] * values[k][b:b + 1, :]
                )
        store_s(l).start()
        load_wo(l).wait()

        def n_wait(d):
            src = lax.rem(me_dp + dp - d, dp)
            remote(
                na.at[l, src], na.at[l, src], n_s.at[l, d], n_r.at[l, src], "dp", src
            ).wait_recv()

        each(dp, n_wait)
        for j in range(dp):
            nf[j * seqs:(j + 1) * seqs, :] = na[l, j].astype(F32)
        mixed = jnp.dot(nf[...].astype(BF16), wo_v[l], preferred_element_type=F32)

        if l == 0:
            ar[me_tp] = mixed.astype(BF16)

            def ar_copy(d):
                return remote(
                    ar.at[me_tp], ar.at[me_tp], ar_s.at[d], ar_r.at[me_tp], "tp",
                    lax.rem(me_tp + d, tp),
                )

            each(tp, lambda d: ar_copy(d).start())

            def ar_wait(d):
                src = lax.rem(me_tp + tp - d, tp)
                remote(
                    ar.at[src], ar.at[src], ar_s.at[d], ar_r.at[src], "tp", src
                ).wait_recv()

            each(tp, ar_wait)
            acc = ar[0].astype(F32)
            for j in range(1, tp):
                acc = acc + ar[j].astype(F32)
            hf[...] = (hf[...] + acc).astype(BF16).astype(F32)
            for j in range(tp):
                h3[j] = hf[j * rows:(j + 1) * rows, :]
        else:
            po[...] = mixed
            for j in range(tp):
                rs[j] = po[j * rows:(j + 1) * rows, :].astype(BF16)

            def rs_copy(d):
                peer = lax.rem(me_tp + d, tp)
                return remote(
                    rs.at[peer], rr.at[me_tp], rs_s.at[d], rs_r.at[me_tp], "tp", peer
                )

            each(tp, lambda d: rs_copy(d).start())
            rr[me_tp] = rs[me_tp]

            def rs_wait(d):
                src = lax.rem(me_tp + tp - d, tp)
                remote(rs.at[src], rr.at[src], rs_s.at[d], rs_r.at[src], "tp", src).wait_recv()

            each(tp, rs_wait)
            acc = rr[0].astype(F32)
            for j in range(1, tp):
                acc = acc + rr[j].astype(F32)
            out[...] = (h3[me_tp] + acc).astype(BF16)
            each(tp, lambda d: rs_copy(d).wait_send())
            each(tp, lambda d: ar_copy(d).wait_send())
        each(dp, lambda d: sq_copy(d).wait_send())
        for i in range(4):
            each(dp, lambda d: p_copy(i, d).wait_send())
        each(dp, lambda d: n_copy(d).wait_send())
    each(tp, lambda d: xg_copy(d).wait_send())
    for l in range(2):
        store_s(l).wait()


def per_device(
    tp, dp,
    tokens, norm_gain, w_query, w_forget, w_value, w_gate, lower_bound, head_gain, w_out, state
):
    rows, cols = tokens.shape
    seqs = state.shape[1]
    heads = state.shape[2]
    width = w_query.shape[2]
    batch = rows * tp
    pad = -(-2 * seqs * heads // LANES) * LANES
    vmem = pl.BlockSpec(memory_space=pltpu.VMEM)
    hbm = pl.BlockSpec(memory_space=pl.ANY)
    dma = pltpu.SemaphoreType.DMA
    return pl.pallas_call(
        functools.partial(kernel, tp, dp),
        name="two_blocks",
        out_shape=(
            jax.ShapeDtypeStruct(tokens.shape, BF16),
            jax.ShapeDtypeStruct(state.shape, F32),
        ),
        in_specs=[vmem, vmem, hbm, hbm, hbm, hbm, vmem, vmem, hbm, hbm],
        out_specs=(vmem, hbm),
        scratch_shapes=[
            pltpu.VMEM((2, 4, cols, width), BF16),
            pltpu.VMEM((2, width, cols), BF16),
            pltpu.VMEM(state.shape, F32),
            pltpu.VMEM((tp, rows, cols), BF16),
            pltpu.VMEM((batch, cols), F32),
            pltpu.VMEM((tp, rows, cols), F32),
            pltpu.VMEM((batch, LANES), F32),
            pltpu.VMEM((2, dp, seqs, LANES), F32),
            pltpu.VMEM((2, dp, seqs, LANES), F32),
            pltpu.VMEM((4, batch, width), F32),
            pltpu.VMEM((2, 4, dp, seqs, width), BF16),
            pltpu.VMEM((2, 4, dp, seqs, width), BF16),
            pltpu.VMEM((pad, LANES), F32),
            pltpu.VMEM((pad, LANES), F32),
            pltpu.VMEM((max(8, seqs * heads), LANES), F32),
            pltpu.VMEM((2, dp, seqs, width), BF16),
            pltpu.VMEM((batch, width), F32),
            pltpu.VMEM((batch, cols), F32),
            pltpu.VMEM((tp, batch, cols), BF16),
            pltpu.VMEM((tp, rows, cols), BF16),
            pltpu.VMEM((tp, rows, cols), BF16),
            dma((2, 4)), dma((2,)), dma((2,)), dma((2,)),
            dma((tp,)), dma((tp,)),
            dma((2, dp)), dma((2, dp)),
            dma((2, 4, dp)), dma((2, 4, dp)),
            dma((2, dp)), dma((2, dp)),
            dma((tp,)), dma((tp,)), dma((tp,)), dma((tp,)),
        ],
        compiler_params=pltpu.CompilerParams(
            collective_id=0, has_side_effects=True, vmem_limit_bytes=60 * 1024 * 1024
        ),
    )(tokens, norm_gain, w_query, w_forget, w_value, w_gate, lower_bound, head_gain, w_out, state)


def solution(mesh):
    return jax.shard_map(
        functools.partial(per_device, mesh.shape["tp"], mesh.shape["dp"]),
        mesh=mesh,
        in_specs=(
            P(("grp", "tp"), "dp"),
            P(None, "dp"),
            P(None, "dp", "tp"),
            P(None, "dp", "tp"),
            P(None, "dp", "tp"),
            P(None, "dp", "tp"),
            P(None, "tp"),
            P(),
            P(None, "tp", "dp"),
            P(None, ("grp", "dp"), "tp", None, None),
        ),
        out_specs=(P(("grp", "tp"), "dp"), P(None, ("grp", "dp"), "tp", None, None)),
        check_vma=False,
    )
```

time: 182 us -> 39.3 us (0.22)
  blocking collectives: 88.1 us -> 0 us
  waiting for transfers between devices: 54.5 us -> 0 us
  Pallas kernels: 0 us -> 33.9 us
  between operations: 14.9 us -> 0.64 us
  matrix products: 14.1 us -> 0 us
  other arithmetic: 8.64 us -> 0 us
  local copies, waits for them, and re-layouts: 1.65 us -> 4.44 us
    psum x2 -> x0, waiting for transfers between devices: 54.4 us -> none  [per_device(): lax.psum(payload[0].astype(jnp.bfloat16), 'dp').astype(jnp.float32)]
    all_gather x4 -> x0, blocking collectives: 38.6 us -> none  [the longest x2 28.2 us: per_device(): gathered = lax.all_gather(hidden, 'tp', axis=0, tiled=True)]
    unnamed x2 -> x0, blocking collectives: 38 us -> none
    pallas_call x0 -> x1, Pallas kernels: none -> 33.9 us  [per_device(): pl.pallas_call(functools.partial(kernel, tp, dp), name='two_blocks', out_...]
    dot_general x12 -> x0, matrix products: 14.1 us -> none  [the longest x8 8.47 us: per_device(): jnp.dot(scaled, weight[layer], preferred_element_type=jnp.float32)]
    psum x2 -> x0, blocking collectives: 11.5 us -> none  [per_device(): square_total = lax.psum(squares, 'dp')]
    unnamed x19 -> x2, local copies, waits for them, and re-layouts: 0.65 us -> 4.44 us
    add x3 -> x0, other arithmetic: 2.78 us -> none  [the longest x1 2.6 us: per_device(): shaped(forget)[..., None] * state[layer]]
  transfers between devices with their start and end apart: 2 -> 0, of which waited for: 2 -> 0; matrix products, arithmetic and copies ran while one was open for 0% -> 0% of each run, Pallas kernels for 0% -> 0%
where the time goes in v1:
time: 39.3 us; the launch traced here: 39 us
  Pallas kernels  33.9 us (86%)
  local copies, waits for them, and re-layouts  4.44 us (11%)
  between operations  0.64 us (2%)
    pallas_call x1, Pallas kernels, per_device(): pl.pallas_call(functools.partial(kernel, tp, dp), name='two_blocks', out_...  33.9 us
    unnamed x2, local copies, waits for them, and re-layouts  4.44 us

profile of v1, /device:TPU:0, one launch (start us, length us, event | category | flops | bytes accessed | tf_op | source)
XLA Modules:
  0.0 39.0 jit_solution(2348905308792388215)
XLA Ops:
  0.6 33.9 %two_blocks.1 = (bf16[4,1024]{1,0:T(4,128)(2,1)}, f32[2,4,4,128,128]{4,3,2,1,0:T(8,128)}) custom-call(bf16[4,1024]{1,0:T(4,128)(2,1)} %tok.1, f32[2,1024]{1,0:T(2,128)} %gain.1, bf16[2,1024,512]{2,1,0:T(8,128)(2,1)} %wq.1, bf16[2,1024,512]{2,1,0:T(8,128)(2,1)} %wf.1, bf16[2,1024,512]{2,1,0:T(8,128)(2,1)} %wv.1, bf16[2,1024,512]{2,1,0:T(8,128)(2,1)} %wg.1, ...), custom_call_target="tpu_custom_call" | custom-call | tf_op jit(solution)/shard_map/two_blocks/pallas_call | solution.py:290
  34.5 1.3 %copy.14 = bf16[4,1024]{1,0:T(4,128)(2,1)} copy(bf16[4,1024]{1,0:T(4,128)(2,1)} %get-tuple-element.4) | data formatting | bytes 16384
  35.8 3.1 %copy.15 = f32[2,4,4,128,128]{4,3,2,1,0:T(8,128)} copy(f32[2,4,4,128,128]{4,3,2,1,0:T(8,128)} %get-tuple-element.5) | data formatting | bytes 4194304

commit v2 on v1

--- a/solution.py
+++ b/solution.py
@@ -10,6 +10,7 @@
 MESH = pl.DeviceIdType.MESH
 LANES = 128
 F32 = jnp.float32
+GROUPS = 2
 BF16 = jnp.bfloat16
 
 
@@ -26,11 +27,11 @@
 
 def kernel(
     tp, dp,
-    tok, gain, wq, wf, wv, wg, bound_ref, head_gain, wo, st,
-    out, ns,
-    w_v, wo_v, s_v, xg, hf, h3, sq2, sqs, sqr, pf, ps, pr, tr_a, tr_b, ro,
+    tok_h, gain_h, wq, wf, wv, wg, bound_h, head_gain_h, wo, st,
+    out, s_v,
+    tok, gain, bound_ref, head_gain, w_v, wo_v, xg, hf, h3, sq2, sqs, sqr, pf, ps, pr, tr_a, tr_b, ro,
     na, nf, po, ar, rs, rr,
-    w_sem, wo_sem, s_sem, o_sem, xg_s, xg_r, sq_s, sq_r, p_s, p_r, n_s, n_r,
+    small_sem, w_sem, wo_sem, s_sem, xg_s, xg_r, sq_s, sq_r, p_s, p_r, n_s, n_r,
     ar_s, ar_r, rs_s, rs_r,
 ):
     rows, cols = tok.shape
@@ -58,29 +59,35 @@
     def load_s(l):
         return pltpu.make_async_copy(st.at[l], s_v.at[l], s_sem.at[l])
 
-    def store_s(l):
-        return pltpu.make_async_copy(s_v.at[l], ns.at[l], o_sem.at[l])
-
+    smalls = [
+        pltpu.make_async_copy(src, dst, small_sem.at[i])
+        for i, (src, dst) in enumerate(
+            ((tok_h, tok), (gain_h, gain), (bound_h, bound_ref), (head_gain_h, head_gain))
+        )
+    ]
+    smalls[0].start()
+    barrier = pltpu.get_barrier_semaphore()
+
+    def greet_tp(d):
+        pl.semaphore_signal(
+            barrier, inc=1, device_id={"tp": lax.rem(me_tp + d, tp)}, device_id_type=MESH
+        )
+
+    def greet_dp(d):
+        pl.semaphore_signal(
+            barrier, inc=1, device_id={"dp": lax.rem(me_dp + d, dp)}, device_id_type=MESH
+        )
+
+    each(tp, greet_tp)
+    each(dp, greet_dp)
+    for copy in smalls[1:]:
+        copy.start()
     for l in range(2):
         for i in range(4):
             load_w(l, i).start()
         load_s(l).start()
         load_wo(l).start()
-
-    barrier = pltpu.get_barrier_semaphore()
-
-    def greet_tp(d):
-        pl.semaphore_signal(
-            barrier, inc=1, device_id={"tp": lax.rem(me_tp + d, tp)}, device_id_type=MESH
-        )
-
-    def greet_dp(d):
-        pl.semaphore_signal(
-            barrier, inc=1, device_id={"dp": lax.rem(me_dp + d, dp)}, device_id_type=MESH
-        )
-
-    each(tp, greet_tp)
-    each(dp, greet_dp)
+    smalls[0].wait()
     pl.semaphore_wait(barrier, tp + dp - 2)
 
     def xg_copy(d):
@@ -97,6 +104,8 @@
     for j in range(tp):
         hf[j * rows:(j + 1) * rows, :] = xg[j].astype(F32)
 
+    for copy in smalls[1:]:
+        copy.wait()
     for l in range(2):
         h = hf[...]
         sq2[...] = jnp.broadcast_to(
@@ -121,12 +130,15 @@
                 "dp", peer,
             )
 
+        per = 4 // GROUPS
         for i in range(4):
             load_w(l, i).wait()
             pf[i] = jnp.dot(scaled, w_v[l, i], preferred_element_type=F32)
+            part = slice(i % per * width, (i % per + 1) * width)
             for j in range(dp):
-                ps[l, i, j] = pf[i, j * seqs:(j + 1) * seqs, :].astype(BF16)
-            each(dp, lambda d: p_copy(i, d).start())
+                ps[l, i // per, j, :, part] = pf[i, j * seqs:(j + 1) * seqs, :].astype(BF16)
+            if i % per == per - 1:
+                each(dp, lambda d: p_copy(i // per, d).start())
 
         def sq_wait(d):
             src = lax.rem(me_dp + dp - d, dp)
@@ -143,7 +155,7 @@
 
         load_s(l).wait()
         proj = []
-        for i in range(4):
+        for i in range(GROUPS):
 
             def p_wait(d):
                 src = lax.rem(me_dp + dp - d, dp)
@@ -157,7 +169,7 @@
             acc = pr[l, i, 0].astype(F32)
             for j in range(1, dp):
                 acc = acc + pr[l, i, j].astype(F32)
-            proj.append(acc)
+            proj.extend(acc[:, g * width:(g + 1) * width] for g in range(per))
 
         values, dots, gates = [], [], []
         for k in range(heads):
@@ -202,7 +214,6 @@
                     cols_b[:, p:p + 1] * s_v[l, b, k]
                     + cols_b[:, pairs + p:pairs + p + 1] * values[k][b:b + 1, :]
                 )
-        store_s(l).start()
         load_wo(l).wait()
 
         def n_wait(d):
@@ -266,12 +277,10 @@
             each(tp, lambda d: rs_copy(d).wait_send())
             each(tp, lambda d: ar_copy(d).wait_send())
         each(dp, lambda d: sq_copy(d).wait_send())
-        for i in range(4):
+        for i in range(GROUPS):
             each(dp, lambda d: p_copy(i, d).wait_send())
         each(dp, lambda d: n_copy(d).wait_send())
     each(tp, lambda d: xg_copy(d).wait_send())
-    for l in range(2):
-        store_s(l).wait()
 
 
 def per_device(
@@ -285,7 +294,7 @@
     batch = rows * tp
     pad = -(-2 * seqs * heads // LANES) * LANES
     vmem = pl.BlockSpec(memory_space=pltpu.VMEM)
-    hbm = pl.BlockSpec(memory_space=pl.ANY)
+    hbm = pl.BlockSpec(memory_space=pltpu.HBM)
     dma = pltpu.SemaphoreType.DMA
     return pl.pallas_call(
         functools.partial(kernel, tp, dp),
@@ -294,12 +303,15 @@
             jax.ShapeDtypeStruct(tokens.shape, BF16),
             jax.ShapeDtypeStruct(state.shape, F32),
         ),
-        in_specs=[vmem, vmem, hbm, hbm, hbm, hbm, vmem, vmem, hbm, hbm],
-        out_specs=(vmem, hbm),
+        in_specs=[hbm] * 10,
+        out_specs=(vmem, vmem),
         scratch_shapes=[
+            pltpu.VMEM(tokens.shape, BF16),
+            pltpu.VMEM(norm_gain.shape, F32),
+            pltpu.VMEM(lower_bound.shape, F32),
+            pltpu.VMEM(head_gain.shape, F32),
             pltpu.VMEM((2, 4, cols, width), BF16),
             pltpu.VMEM((2, width, cols), BF16),
-            pltpu.VMEM(state.shape, F32),
             pltpu.VMEM((tp, rows, cols), BF16),
             pltpu.VMEM((batch, cols), F32),
             pltpu.VMEM((tp, rows, cols), F32),
@@ -307,8 +319,8 @@
             pltpu.VMEM((2, dp, seqs, LANES), F32),
             pltpu.VMEM((2, dp, seqs, LANES), F32),
             pltpu.VMEM((4, batch, width), F32),
-            pltpu.VMEM((2, 4, dp, seqs, width), BF16),
-            pltpu.VMEM((2, 4, dp, seqs, width), BF16),
+            pltpu.VMEM((2, GROUPS, dp, seqs, 4 // GROUPS * width), BF16),
+            pltpu.VMEM((2, GROUPS, dp, seqs, 4 // GROUPS * width), BF16),
             pltpu.VMEM((pad, LANES), F32),
             pltpu.VMEM((pad, LANES), F32),
             pltpu.VMEM((max(8, seqs * heads), LANES), F32),
@@ -318,17 +330,23 @@
             pltpu.VMEM((tp, batch, cols), BF16),
             pltpu.VMEM((tp, rows, cols), BF16),
             pltpu.VMEM((tp, rows, cols), BF16),
-            dma((2, 4)), dma((2,)), dma((2,)), dma((2,)),
+            dma((4,)), dma((2, 4)), dma((2,)), dma((2,)),
             dma((tp,)), dma((tp,)),
             dma((2, dp)), dma((2, dp)),
-            dma((2, 4, dp)), dma((2, 4, dp)),
+            dma((2, GROUPS, dp)), dma((2, GROUPS, dp)),
             dma((2, dp)), dma((2, dp)),
             dma((tp,)), dma((tp,)), dma((tp,)), dma((tp,)),
         ],
         compiler_params=pltpu.CompilerParams(
-            collective_id=0, has_side_effects=True, vmem_limit_bytes=60 * 1024 * 1024
+            collective_id=0, has_side_effects=True, vmem_limit_bytes=32 * 1024 * 1024
         ),
-    )(tokens, norm_gain, w_query, w_forget, w_value, w_gate, lower_bound, head_gain, w_out, state)
+    )(*(
+        pltpu.with_memory_space_constraint(array, pltpu.HBM)
+        for array in (
+            tokens, norm_gain, w_query, w_forget, w_value, w_gate, lower_bound, head_gain, w_out,
+            state,
+        )
+    ))
 
 
 def solution(mesh):

time: 39.3 us -> 35.2 us (0.90)
  local copies, waits for them, and re-layouts: 4.44 us -> 1.92 us
  Pallas kernels: 33.9 us -> 32.4 us
    unnamed x2, local copies, waits for them, and re-layouts: 4.44 us -> 1.92 us
    pallas_call x1, Pallas kernels: 33.9 us -> 32.4 us  [per_device(): pl.pallas_call(functools.partial(kernel, tp, dp), name='two_blocks', out_...]
where the time goes in v2:
time: 35.2 us; the launch traced here: 35 us
  Pallas kernels  32.4 us (92%)
  local copies, waits for them, and re-layouts  1.92 us (5%)
  between operations  0.64 us (2%)
    pallas_call x1, Pallas kernels, per_device(): pl.pallas_call(functools.partial(kernel, tp, dp), name='two_blocks', out_...  32.4 us
    unnamed x2, local copies, waits for them, and re-layouts  1.92 us

profile of v2, /device:TPU:0, one launch (start us, length us, event | category | flops | bytes accessed | tf_op | source)
XLA Modules:
  0.0 35.0 jit_solution(2361831273499104516)
XLA Ops:
  0.6 32.4 %two_blocks.1 = (bf16[4,1024]{1,0:T(4,128)(2,1)S(1)}, f32[2,4,4,128,128]{4,3,2,1,0:T(8,128)S(1)}) custom-call(bf16[4,1024]{1,0:T(4,128)(2,1)} %tok_h.1, f32[2,1024]{1,0:T(2,128)} %gain_h.1, bf16[2,1024,512]{2,1,0:T(8,128)(2,1)} %wq.1, bf16[2,1024,512]{2,1,0:T(8,128)(2,1)} %wf.1, bf16[2,1024,512]{2,1,0:T(8,128)(2,1)} %wv.1, bf16[2,1024,512]{2,1,0:T(8,128)(2,1)} %wg.1, ...), custom_call_target="tpu_custom_call" | custom-call | tf_op jit(solution)/shard_map/two_blocks/pallas_call | solution.py:299
  33.1 0.6 %copy.14 = bf16[4,1024]{1,0:T(4,128)(2,1)} copy(bf16[4,1024]{1,0:T(4,128)(2,1)S(1)} %get-tuple-element.4) | data formatting | bytes 16384
  33.7 1.3 %copy.15 = f32[2,4,4,128,128]{4,3,2,1,0:T(8,128)} copy(f32[2,4,4,128,128]{4,3,2,1,0:T(8,128)S(1)} %get-tuple-element.5) | data formatting | bytes 4194304

commit v3 on v2

--- a/solution.py
+++ b/solution.py
@@ -48,6 +48,10 @@
             device_id={axis: peer}, device_id_type=MESH,
         )
 
+    def far(k):
+        above = tp - me_tp
+        return jnp.where(k < above, tp - k, k - above)
+
     weights = (wq, wf, wv, wg)
 
     def load_w(l, i):
@@ -91,7 +95,7 @@
     pl.semaphore_wait(barrier, tp + dp - 2)
 
     def xg_copy(d):
-        return remote(tok, xg.at[me_tp], xg_s.at[d], xg_r.at[me_tp], "tp", lax.rem(me_tp + d, tp))
+        return remote(tok, xg.at[me_tp], xg_s.at[d], xg_r.at[me_tp], "tp", far(d))
 
     each(tp, lambda d: xg_copy(d).start())
     xg[me_tp] = tok[...]
@@ -233,7 +237,7 @@
             def ar_copy(d):
                 return remote(
                     ar.at[me_tp], ar.at[me_tp], ar_s.at[d], ar_r.at[me_tp], "tp",
-                    lax.rem(me_tp + d, tp),
+                    far(d),
                 )
 
             each(tp, lambda d: ar_copy(d).start())
@@ -257,7 +261,7 @@
                 rs[j] = po[j * rows:(j + 1) * rows, :].astype(BF16)
 
             def rs_copy(d):
-                peer = lax.rem(me_tp + d, tp)
+                peer = far(d)
                 return remote(
                     rs.at[peer], rr.at[me_tp], rs_s.at[d], rs_r.at[me_tp], "tp", peer
                 )

time: 35.2 us -> 34.4 us (0.977)
  Pallas kernels: 32.4 us -> 31.6 us
    pallas_call x1, Pallas kernels: 32.4 us -> 31.6 us  [per_device(): pl.pallas_call(functools.partial(kernel, tp, dp), name='two_blocks', out_...]
where the time goes in v3:
time: 34.4 us; the launch traced here: 34.2 us
  Pallas kernels  31.6 us (92%)
  local copies, waits for them, and re-layouts  1.92 us (6%)
  between operations  0.64 us (2%)
    pallas_call x1, Pallas kernels, per_device(): pl.pallas_call(functools.partial(kernel, tp, dp), name='two_blocks', out_...  31.6 us
    unnamed x2, local copies, waits for them, and re-layouts  1.92 us

profile of v3, /device:TPU:0, one launch (start us, length us, event | category | flops | bytes accessed | tf_op | source)
XLA Modules:
  0.0 34.2 jit_solution(4231204476735121931)
XLA Ops:
  0.6 31.6 %two_blocks.1 = (bf16[4,1024]{1,0:T(4,128)(2,1)S(1)}, f32[2,4,4,128,128]{4,3,2,1,0:T(8,128)S(1)}) custom-call(bf16[4,1024]{1,0:T(4,128)(2,1)} %tok_h.1, f32[2,1024]{1,0:T(2,128)} %gain_h.1, bf16[2,1024,512]{2,1,0:T(8,128)(2,1)} %wq.1, bf16[2,1024,512]{2,1,0:T(8,128)(2,1)} %wf.1, bf16[2,1024,512]{2,1,0:T(8,128)(2,1)} %wv.1, bf16[2,1024,512]{2,1,0:T(8,128)(2,1)} %wg.1, ...), custom_call_target="tpu_custom_call" | custom-call | tf_op jit(solution)/shard_map/two_blocks/pallas_call | solution.py:303
  32.3 0.6 %copy.14 = bf16[4,1024]{1,0:T(4,128)(2,1)} copy(bf16[4,1024]{1,0:T(4,128)(2,1)S(1)} %get-tuple-element.4) | data formatting | bytes 16384
  32.9 1.3 %copy.15 = f32[2,4,4,128,128]{4,3,2,1,0:T(8,128)} copy(f32[2,4,4,128,128]{4,3,2,1,0:T(8,128)S(1)} %get-tuple-element.5) | data formatting | bytes 4194304

commit v4 on v3

--- a/solution.py
+++ b/solution.py
@@ -38,6 +38,7 @@
     seqs, heads, hd = st.shape[1], st.shape[2], st.shape[3]
     width = wq.shape[2]
     pairs = seqs * heads
+    chunks = ar.shape[0]
     features = cols * dp
     me_tp = lax.axis_index("tp")
     me_dp = lax.axis_index("dp")
@@ -111,10 +112,27 @@
     for copy in smalls[1:]:
         copy.wait()
     for l in range(2):
-        h = hf[...]
-        sq2[...] = jnp.broadcast_to(
-            jnp.sum(h * h, axis=1, keepdims=True), (h.shape[0], LANES)
-        )
+        steps = chunks if l else 1
+        step = cols // steps
+        squares = 0.0
+        for c in range(steps):
+            at = slice(c * step, (c + 1) * step)
+            if l:
+                each(tp, lambda d: ar_copy(c, d, True).wait_recv())
+                acc = ar[c, 0].astype(F32)
+                for j in range(1, tp):
+                    acc = acc + ar[c, j].astype(F32)
+                hf[:, at] = (hf[:, at] + acc).astype(BF16).astype(F32)
+            h = hf[:, at]
+            squares = squares + jnp.sum(h * h, axis=1, keepdims=True)
+            scaled = (h * gain[l:l + 1, at]).astype(BF16)
+            if c < steps - 1:
+                for i in range(4):
+                    if c == 0:
+                        load_w(l, i).wait()
+                    part = jnp.dot(scaled, w_v[l, i, at, :], preferred_element_type=F32)
+                    pf[i] = part if c == 0 else pf[i] + part
+        sq2[...] = jnp.broadcast_to(squares, (squares.shape[0], LANES))
         for j in range(dp):
             sqs[l, j] = sq2[j * seqs:(j + 1) * seqs, :]
 
@@ -125,7 +143,6 @@
             )
 
         each(dp, lambda d: sq_copy(d).start())
-        scaled = (h * gain[l:l + 1, :]).astype(BF16)
 
         def p_copy(i, d):
             peer = lax.rem(me_dp + d, dp)
@@ -136,8 +153,10 @@
 
         per = 4 // GROUPS
         for i in range(4):
-            load_w(l, i).wait()
-            pf[i] = jnp.dot(scaled, w_v[l, i], preferred_element_type=F32)
+            if steps == 1:
+                load_w(l, i).wait()
+            rest = jnp.dot(scaled, w_v[l, i, at, :], preferred_element_type=F32)
+            pf[i] = rest if steps == 1 else pf[i] + rest
             part = slice(i % per * width, (i % per + 1) * width)
             for j in range(dp):
                 ps[l, i // per, j, :, part] = pf[i, j * seqs:(j + 1) * seqs, :].astype(BF16)
@@ -229,34 +248,28 @@
         each(dp, n_wait)
         for j in range(dp):
             nf[j * seqs:(j + 1) * seqs, :] = na[l, j].astype(F32)
-        mixed = jnp.dot(nf[...].astype(BF16), wo_v[l], preferred_element_type=F32)
+        gathered = nf[...].astype(BF16)
 
         if l == 0:
-            ar[me_tp] = mixed.astype(BF16)
-
-            def ar_copy(d):
+
+            def ar_copy(c, d, incoming=False):
+                src = lax.rem(me_tp + tp - d, tp) if incoming else me_tp
                 return remote(
-                    ar.at[me_tp], ar.at[me_tp], ar_s.at[d], ar_r.at[me_tp], "tp",
-                    far(d),
+                    ar.at[c, src], ar.at[c, src], ar_s.at[c, d], ar_r.at[c, src], "tp",
+                    src if incoming else far(d),
                 )
 
-            each(tp, lambda d: ar_copy(d).start())
-
-            def ar_wait(d):
-                src = lax.rem(me_tp + tp - d, tp)
-                remote(
-                    ar.at[src], ar.at[src], ar_s.at[d], ar_r.at[src], "tp", src
-                ).wait_recv()
-
-            each(tp, ar_wait)
-            acc = ar[0].astype(F32)
-            for j in range(1, tp):
-                acc = acc + ar[j].astype(F32)
-            hf[...] = (hf[...] + acc).astype(BF16).astype(F32)
+            for c in range(chunks):
+                ar[c, me_tp] = jnp.dot(
+                    gathered,
+                    wo_v[l, :, c * (cols // chunks):(c + 1) * (cols // chunks)],
+                    preferred_element_type=F32,
+                ).astype(BF16)
+                each(tp, lambda d: ar_copy(c, d).start())
+        else:
             for j in range(tp):
                 h3[j] = hf[j * rows:(j + 1) * rows, :]
-        else:
-            po[...] = mixed
+            po[...] = jnp.dot(gathered, wo_v[l], preferred_element_type=F32)
             for j in range(tp):
                 rs[j] = po[j * rows:(j + 1) * rows, :].astype(BF16)
 
@@ -279,7 +292,8 @@
                 acc = acc + rr[j].astype(F32)
             out[...] = (h3[me_tp] + acc).astype(BF16)
             each(tp, lambda d: rs_copy(d).wait_send())
-            each(tp, lambda d: ar_copy(d).wait_send())
+            for c in range(chunks):
+                each(tp, lambda d: ar_copy(c, d).wait_send())
         each(dp, lambda d: sq_copy(d).wait_send())
         for i in range(GROUPS):
             each(dp, lambda d: p_copy(i, d).wait_send())
@@ -296,6 +310,7 @@
     heads = state.shape[2]
     width = w_query.shape[2]
     batch = rows * tp
+    chunks = 2 if cols % (2 * LANES) == 0 else 1
     pad = -(-2 * seqs * heads // LANES) * LANES
     vmem = pl.BlockSpec(memory_space=pltpu.VMEM)
     hbm = pl.BlockSpec(memory_space=pltpu.HBM)
@@ -331,7 +346,7 @@
             pltpu.VMEM((2, dp, seqs, width), BF16),
             pltpu.VMEM((batch, width), F32),
             pltpu.VMEM((batch, cols), F32),
-            pltpu.VMEM((tp, batch, cols), BF16),
+            pltpu.VMEM((chunks, tp, batch, cols // chunks), BF16),
             pltpu.VMEM((tp, rows, cols), BF16),
             pltpu.VMEM((tp, rows, cols), BF16),
             dma((4,)), dma((2, 4)), dma((2,)), dma((2,)),
@@ -339,7 +354,7 @@
             dma((2, dp)), dma((2, dp)),
             dma((2, GROUPS, dp)), dma((2, GROUPS, dp)),
             dma((2, dp)), dma((2, dp)),
-            dma((tp,)), dma((tp,)), dma((tp,)), dma((tp,)),
+            dma((chunks, tp)), dma((chunks, tp)), dma((tp,)), dma((tp,)),
         ],
         compiler_params=pltpu.CompilerParams(
             collective_id=0, has_side_effects=True, vmem_limit_bytes=32 * 1024 * 1024

time: 34.4 us -> 34.3 us (level)
  no operation moved by 1% of the time
where the time goes in v4:
time: 34.3 us; the launch traced here: 34.1 us
  Pallas kernels  31.5 us (92%)
  local copies, waits for them, and re-layouts  1.92 us (6%)
  between operations  0.64 us (2%)
    pallas_call x1, Pallas kernels, per_device(): pl.pallas_call(functools.partial(kernel, tp, dp), name='two_blocks', out_...  31.5 us
    unnamed x2, local copies, waits for them, and re-layouts  1.92 us

profile of v4, /device:TPU:0, one launch (start us, length us, event | category | flops | bytes accessed | tf_op | source)
XLA Modules:
  0.0 34.1 jit_solution(12171963430420561285)
XLA Ops:
  0.6 31.5 %two_blocks.1 = (bf16[4,1024]{1,0:T(4,128)(2,1)S(1)}, f32[2,4,4,128,128]{4,3,2,1,0:T(8,128)S(1)}) custom-call(bf16[4,1024]{1,0:T(4,128)(2,1)} %tok_h.1, f32[2,1024]{1,0:T(2,128)} %gain_h.1, bf16[2,1024,512]{2,1,0:T(8,128)(2,1)} %wq.1, bf16[2,1024,512]{2,1,0:T(8,128)(2,1)} %wf.1, bf16[2,1024,512]{2,1,0:T(8,128)(2,1)} %wv.1, bf16[2,1024,512]{2,1,0:T(8,128)(2,1)} %wg.1, ...), custom_call_target="tpu_custom_call" | custom-call | tf_op jit(solution)/shard_map/two_blocks/pallas_call | solution.py:318
  32.2 0.6 %copy.14 = bf16[4,1024]{1,0:T(4,128)(2,1)} copy(bf16[4,1024]{1,0:T(4,128)(2,1)S(1)} %get-tuple-element.4) | data formatting | bytes 16384
  32.8 1.3 %copy.15 = f32[2,4,4,128,128]{4,3,2,1,0:T(8,128)} copy(f32[2,4,4,128,128]{4,3,2,1,0:T(8,128)S(1)} %get-tuple-element.5) | data formatting | bytes 4194304
